TPU v7x, 32 devices: a whole 2x2x4 slice. The times are simulated.
32 devices in a mesh: fs: 8 (over z, y), tp: 4 (over x, core).
Axes of the slice: x: 2, y: 2, z: 4, core: 2. Of those that a mesh axis runs over, the one named last changes fastest.
Arguments:
- h_saved: bfloat16 [4096, 4096], P('fs'), may hold values from -8 to 8
- y_saved: bfloat16 [4096, 2048], P('fs'), may hold values from -8 to 8
- d_gate: bfloat16 [4096, 2048], P('fs', 'tp'), may hold values from -0.25 to 0.25
- d_out: bfloat16 [4096, 4096], P('fs', 'tp'), may hold values from -0.25 to 0.25
- p_gate: bfloat16 [4096, 256], P('fs'), may hold values from -2 to 2
- p_out: bfloat16 [2048, 256], P('fs'), may hold values from -2 to 2
- w_gate: float32 [4096, 2048], P('fs', 'tp'), may hold values from -6 to 6
- w_out: float32 [2048, 4096], P('fs', 'tp'), may hold values from -6 to 6
- m_gate: float32 [256, 2048], P('fs', 'tp'), may hold values from -4 to 4
- m_out: float32 [256, 4096], P('fs', 'tp'), may hold values from -4 to 4
- v_gate: float32 [256, 2048], P('fs', 'tp'), may hold values from 0.02 to 0.2
- v_out: float32 [256, 4096], P('fs', 'tp'), may hold values from 0.02 to 0.2
Outputs:
- step_gate: float32 [4096, 2048], P('fs', 'tp')
- step_out: float32 [2048, 4096], P('fs', 'tp')
- moment_gate: float32 [256, 2048], P('fs', 'tp')
- moment_out: float32 [256, 4096], P('fs', 'tp')
- second_gate: float32 [256, 2048], P('fs', 'tp')
- second_out: float32 [256, 4096], P('fs', 'tp')
- copy_gate: bfloat16 [4096, 2048], P(None, 'tp')
- copy_out: bfloat16 [2048, 4096], P(None, 'tp')
All inputs are finite; a program needn't handle non-finite values.
Results may differ from a plain program's by a relative error of at most 0.001.
Values may be sent and summed in bfloat16 or wider, within the bound.
A program may use at most 64 MiB of HBM per device.

v0:
```python
import jax
import jax.numpy as jnp
from jax import lax
from jax.sharding import PartitionSpec as P

BETA_ONE = 0.9
BETA_TWO = 0.95
LEARN_RATE = 0.1
EPSILON = 1e-06
TOKEN_DIMS = (((0,), (0,)), ((), ()))


def projected_partial(saved, cotangent, factor):
    reduced = jnp.dot(
        saved, lax.all_gather(factor, "fs", axis=0, tiled=True), preferred_element_type=jnp.float32
    )
    return lax.dot_general(
        reduced,
        cotangent.astype(jnp.float32),
        TOKEN_DIMS,
        precision=lax.Precision.HIGHEST,
        preferred_element_type=jnp.float32,
    )


def on_device(
    h_saved, y_saved, d_gate, d_out, p_gate, p_out, w_gate, w_out, m_gate, m_out, v_gate, v_out
):
    part_gate = projected_partial(h_saved, d_gate, p_gate)
    part_out = projected_partial(y_saved, d_out, p_out)
    proj_gate, proj_out = (
        lax.psum_scatter(part_gate, "fs", scatter_dimension=0, tiled=True),
        lax.psum_scatter(part_out, "fs", scatter_dimension=0, tiled=True),
    )
    moment_gate = BETA_ONE * m_gate + (1.0 - BETA_ONE) * proj_gate
    moment_out = BETA_ONE * m_out + (1.0 - BETA_ONE) * proj_out
    second_gate = BETA_TWO * v_gate + (1.0 - BETA_TWO) * proj_gate * proj_gate
    second_out = BETA_TWO * v_out + (1.0 - BETA_TWO) * proj_out * proj_out
    normed_gate = moment_gate / jnp.sqrt(second_gate)
    normed_out = moment_out / jnp.sqrt(second_out)
    whole_gate, whole_out = (
        lax.all_gather(normed_gate, "fs", axis=0, tiled=True),
        lax.all_gather(normed_out, "fs", axis=0, tiled=True),
    )
    update_gate = jnp.dot(p_gate.astype(jnp.float32), whole_gate, precision=lax.Precision.HIGHEST)
    update_out = jnp.dot(p_out.astype(jnp.float32), whole_out, precision=lax.Precision.HIGHEST)
    squares = lax.psum(
        (jnp.sum(update_gate * update_gate), jnp.sum(update_out * update_out)), ("fs", "tp")
    )
    devices_all = lax.axis_size("fs") * lax.axis_size("tp")
    step_gate = update_gate * lax.rsqrt(squares[0] / (update_gate.size * devices_all) + EPSILON)
    step_out = update_out * lax.rsqrt(squares[1] / (update_out.size * devices_all) + EPSILON)
    local_gate = (w_gate - LEARN_RATE * step_gate).astype(jnp.bfloat16)
    local_out = (w_out - LEARN_RATE * step_out).astype(jnp.bfloat16)
    copy_gate, copy_out = (
        lax.all_gather(local_gate, "fs", axis=0, tiled=True),
        lax.all_gather(local_out, "fs", axis=0, tiled=True),
    )
    return (
        step_gate,
        step_out,
        moment_gate,
        moment_out,
        second_gate,
        second_out,
        copy_gate,
        copy_out,
    )


def solution(mesh):
    placed = (
        P("fs", None),
        P("fs", None),
        P("fs", "tp"),
        P("fs", "tp"),
        P("fs", None),
        P("fs", None),
        P("fs", "tp"),
        P("fs", "tp"),
        P("fs", "tp"),
        P("fs", "tp"),
        P("fs", "tp"),
        P("fs", "tp"),
    )
    return jax.shard_map(
        on_device,
        mesh=mesh,
        in_specs=placed,
        out_specs=(
            P("fs", "tp"),
            P("fs", "tp"),
            P("fs", "tp"),
            P("fs", "tp"),
            P("fs", "tp"),
            P("fs", "tp"),
            P(None, "tp"),
            P(None, "tp"),
        ),
        check_vma=False,
    )
```

profile of v0, /device:TPU:0, one launch (start us, length us, event | category | flops | bytes accessed | tf_op | source)
XLA Modules:
  0.0 486.9 jit_solution(17117963242503753305)
XLA Ops:
  7.2 0.0 copy-start
  7.2 0.0 copy-start.1
  7.2 0.0 all-gather.8.cloned.1.call-start
  7.2 0.7 all-gather.8.cloned.1.call-update
  7.9 0.0 all-gather.6.cloned.1.call-start
  8.0 0.7 all-gather.6.cloned.1.call-update
  8.7 0.0 reduce-scatter.5.cloned.1.call-start
  8.7 44.4 %all-gather.8.cloned.1.call-done = bf16[2048,256]{1,0:T(8,128)(2,1)} async-done(((bf16[256,256]{1,0:T(8,128)(2,1)}), bf16[2048,256]{1,0:T(8,128)(2,1)}) %all-gather.8.cloned.1.call-update) | async-done | bytes 1048592 | tf_op jit(solution)/shard_map/all_gather | solution.py:15
  53.2 0.0 copy-done
  53.2 1.9 fusion.6
  55.1 0.0 copy-done.1
  55.1 2.0 fusion.7
  57.1 0.0 reduce-scatter.5.cloned.1.call-update
  57.1 0.0 copy-start.2
  57.2 0.0 reduce-scatter.3.cloned.1.call-start
  57.2 45.9 %all-gather.6.cloned.1.call-done = bf16[4096,256]{1,0:T(8,128)(2,1)} async-done(((bf16[512,256]{1,0:T(8,128)(2,1)}), bf16[4096,256]{1,0:T(8,128)(2,1)}) %all-gather.6.cloned.1.call-update) | async-done | bytes 2097168 | tf_op jit(solution)/shard_map/all_gather | solution.py:15
  103.1 0.0 copy-start.4
  103.1 4.2 fusion.4
  107.3 0.0 copy-done.4
  107.3 0.0 copy-start.3
  107.3 0.0 copy-start.5
  107.3 1.4 fusion.5
  108.7 0.0 reduce-scatter.3.cloned.1.call-update
  108.8 0.0 all-gather.10.cloned.1.call-start
  108.8 61.0 %reduce-scatter.5.cloned.1.call-done = f32[32,1024]{1,0:T(8,128)} async-done(((f32[256,1024]{1,0:T(8,128)}), f32[32,1024]{1,0:T(8,128)}) %reduce-scatter.5.cloned.1.call-update) | async-done | bytes 131088 | tf_op jit(solution)/shard_map/reduce_scatter | solution.py:33
  169.8 1.8 rsqrt_multiply_fusion
  171.6 0.0 all-gather.10.cloned.1.call-update
  171.6 0.0 all-gather.12.cloned.1.call-start
  171.7 0.0 copy-done.2
  171.7 1.3 copy.20
  173.0 62.3 %reduce-scatter.3.cloned.1.call-done = f32[32,512]{1,0:T(8,128)} async-done(((f32[256,512]{1,0:T(8,128)}), f32[32,512]{1,0:T(8,128)}) %reduce-scatter.3.cloned.1.call-update) | async-done | bytes 65552 | tf_op jit(solution)/shard_map/reduce_scatter | solution.py:32
  235.3 1.6 rsqrt_multiply_fusion.1
  236.9 31.7 %all_gather.19 = f32[256,512]{1,0:T(8,128)S(1)} all-gather(f32[32,512]{1,0:T(8,128)S(1)} %get-tuple-element.25), channel_id=1, replica_groups=mesh['fs'=8,'tp'=4] {'fs'}, dimensions={0}, use_global_device_ids=true | all-gather | bytes 589824 | tf_op jit(solution)/shard_map/all_gather | solution.py:42
  268.6 0.0 copy-done.3
  268.6 2.6 multiply_reduce_fusion.1
  271.1 7.3 %all-gather.10.cloned.1.call-done = f32[256,1024]{1,0:T(8,128)} async-done(((f32[32,1024]{1,0:T(8,128)}), f32[256,1024]{1,0:T(8,128)}) %all-gather.10.cloned.1.call-update) | async-done | bytes 1048592 | tf_op jit(solution)/shard_map/all_gather | solution.py:43
  278.4 0.0 copy-done.5
  278.4 2.8 multiply_reduce_fusion
  281.2 38.7 %all-reduce = (f32[]{:T(128)}, f32[]{:T(128)}) all-reduce(f32[]{:T(128)} %get-tuple-element.28, f32[]{:T(128)} %get-tuple-element.30), channel_id=1, replica_groups=mesh['fs'=8,'tp'=4] {'fs','tp'}, use_global_device_ids=true, to_apply=%region_2.0 | all-reduce | flops 2 | bytes 16 | tf_op jit(solution)/shard_map/psum | solution.py:47
  320.6 2.9 subtract_convert_fusion.1
  323.6 0.0 all-gather.12.cloned.1.call-update
  323.6 0.0 all-gather.14.cloned.1.call-start
  323.7 2.5 copy.21
  326.9 2.6 subtract_convert_fusion
  329.4 0.0 all-gather.14.cloned.1.call-update
  329.5 2.5 copy.22
  332.0 2.6 copy.23
  334.6 64.3 %all-gather.12.cloned.1.call-done = bf16[4096,512]{0,1:T(8,128)(2,1)} async-done(((bf16[512,512]{0,1:T(8,128)(2,1)}), bf16[4096,512]{0,1:T(8,128)(2,1)}) %all-gather.12.cloned.1.call-update) | async-done | bytes 4194320 | tf_op jit(solution)/shard_map/all_gather | solution.py:56
  398.8 6.4 %copy.24 = bf16[4096,512]{1,0:T(8,128)(2,1)} copy(bf16[4096,512]{0,1:T(8,128)(2,1)} %all-gather.12.cloned.1.call-done) | data formatting | bytes 8388608
  405.2 68.5 %all-gather.14.cloned.1.call-done = bf16[2048,1024]{0,1:T(8,128)(2,1)} async-done(((bf16[256,1024]{0,1:T(8,128)(2,1)}), bf16[2048,1024]{0,1:T(8,128)(2,1)}) %all-gather.14.cloned.1.call-update) | async-done | bytes 4194320 | tf_op jit(solution)/shard_map/all_gather | solution.py:57
  473.7 6.4 %copy.25 = bf16[2048,1024]{1,0:T(8,128)(2,1)} copy(bf16[2048,1024]{0,1:T(8,128)(2,1)} %all-gather.14.cloned.1.call-done) | data formatting | bytes 8388608
Async XLA Ops:
  7.2 46.0 %copy-start = (bf16[512,2048]{1,0:T(8,128)(2,1)S(1)}, bf16[512,2048]{1,0:T(8,128)(2,1)}, u32[]{:S(2)}) copy-start(bf16[512,2048]{1,0:T(8,128)(2,1)} %param.13) | copy-start | bytes 6291460
  7.2 47.9 %copy-start.1 = (bf16[512,1024]{1,0:T(8,128)(2,1)S(1)}, bf16[512,1024]{1,0:T(8,128)(2,1)}, u32[]{:S(2)}) copy-start(bf16[512,1024]{1,0:T(8,128)(2,1)} %param.15) | copy-start | bytes 3145732
  7.2 46.0 %all-gather.8.cloned.1.call-start = ((), (), s32[]{:S(2)}) async-start(), calls=%async_computation.4 | async-start | bytes 1179648 | tf_op jit(solution)/shard_map/all_gather | solution.py:15
  7.9 95.2 %all-gather.6.cloned.1.call-start = ((), (), s32[]{:S(2)}) async-start(), calls=%async_computation.2 | async-start | bytes 2359296 | tf_op jit(solution)/shard_map/all_gather | solution.py:15
  8.7 161.1 %reduce-scatter.5.cloned.1.call-start = ((), (), s32[]{:S(2)}) async-start(), calls=%async_computation.5 | async-start | bytes 1179648 | tf_op jit(solution)/shard_map/reduce_scatter | solution.py:33
  57.1 114.5 %copy-start.2 = (f32[512,512]{1,0:T(8,128)S(1)}, f32[512,512]{1,0:T(8,128)}, u32[]{:S(2)}) copy-start(f32[512,512]{1,0:T(8,128)} %param.18) | copy-start | bytes 3145732
  57.2 178.1 %reduce-scatter.3.cloned.1.call-start = ((), (), s32[]{:S(2)}) async-start(), calls=%async_computation.3 | async-start | bytes 589824 | tf_op jit(solution)/shard_map/reduce_scatter | solution.py:32
  103.1 4.2 copy-start.4
  107.3 161.3 %copy-start.3 = (bf16[512,256]{1,0:T(8,128)(2,1)S(1)}, bf16[512,256]{1,0:T(8,128)(2,1)}, u32[]{:S(2)}) copy-start(bf16[512,256]{1,0:T(8,128)(2,1)} %param.16) | copy-start | bytes 786436
  107.3 171.1 %copy-start.5 = (bf16[256,256]{1,0:T(8,128)(2,1)S(1)}, bf16[256,256]{1,0:T(8,128)(2,1)}, u32[]{:S(2)}) copy-start(bf16[256,256]{1,0:T(8,128)(2,1)} %param.17) | copy-start | bytes 393220
  108.8 169.6 %all-gather.10.cloned.1.call-start = ((), (), s32[]{:S(2)}) async-start(), calls=%async_computation.6 | async-start | bytes 1179648 | tf_op jit(solution)/shard_map/all_gather | solution.py:43
  171.6 227.2 %all-gather.12.cloned.1.call-start = ((), (), s32[]{:S(2)}) async-start(), calls=%async_computation.7 | async-start | bytes 4718592 | tf_op jit(solution)/shard_map/all_gather | solution.py:56
  323.6 150.1 %all-gather.14.cloned.1.call-start = ((), (), s32[]{:S(2)}) async-start(), calls=%async_computation.8 | async-start | bytes 4718592 | tf_op jit(solution)/shard_map/all_gather | solution.py:57
Sparse Core Ops, SparseCore 0:
  10.1 42.9 all-gather.7
  55.3 47.7 all-gather.5
  107.1 62.6 reduce-scatter.4
  173.6 61.6 reduce-scatter.2
  237.9 40.5 all-gather.9
  323.7 75.0 all-gather.11
  400.9 72.8 all-gather.13
where the time goes:
time: 488 us; the launch traced here: 487 us
  waiting for transfers between devices  355 us (73%)
  blocking collectives  70.4 us (14%)
  local copies, waits for them, and re-layouts  21.8 us (4%)
  between operations  15.6 us (3%)
  matrix products  14.9 us (3%)
  other arithmetic  8.88 us (2%)
    all_gather x2, waiting for transfers between devices, projected_partial(): lax.all_gather(factor, 'fs', axis=0, tiled=True)  90.3 us
    all_gather x1, waiting for transfers between devices, on_device(): lax.all_gather(local_out, 'fs', axis=0, tiled=True)  68.5 us
    all_gather x1, waiting for transfers between devices, on_device(): lax.all_gather(local_gate, 'fs', axis=0, tiled=True)  64.3 us
    reduce_scatter x1, waiting for transfers between devices, on_device(): lax.psum_scatter(part_gate, 'fs', scatter_dimension=0, tiled=True)  62.3 us
    reduce_scatter x1, waiting for transfers between devices, on_device(): lax.psum_scatter(part_out, 'fs', scatter_dimension=0, tiled=True)  61 us
    psum x1, blocking collectives, on_device(): lax.psum((jnp.sum(update_gate * update_gate), jnp.sum(update_out * update...  38.7 us
    all_gather x1, blocking collectives, on_device(): lax.all_gather(normed_gate, 'fs', axis=0, tiled=True)  31.7 us
    unnamed x18, local copies, waits for them, and re-layouts  21.8 us
  transfers between devices with their start and end apart: 7, of which 7 were waited for; matrix products, arithmetic and copies ran while one was open for 7% of the time, Pallas kernels for 0%

commit v1 on v0

v1 whole, which is shorter than its diff:
```python
import functools
import jax
import jax.numpy as jnp
from jax import lax
from jax.experimental import pallas as pl
from jax.experimental.pallas import tpu as pltpu
from jax.sharding import PartitionSpec as P

BETA_ONE = 0.9
BETA_TWO = 0.95
LEARN_RATE = 0.1
EPSILON = 1e-06
MESH = pl.DeviceIdType.MESH
VMEM_SPEC = pl.BlockSpec(memory_space=pltpu.VMEM)
CORES = 2


def grid_of(count):
    inner = 1
    while 4 * inner * inner <= count:
        inner *= 2
    return count // inner, inner


def both(*conditions):
    kept = [c for c in conditions if c is not True]
    if not kept:
        return True
    return functools.reduce(jnp.logical_and, kept)


def when(condition, action):
    if condition is True:
        action()
    else:
        pl.when(condition)(action)


def greet(axis, spots):
    barrier = pltpu.get_barrier_semaphore()
    total = 0
    for valid, index in spots:

        def signal(index=index):
            pl.semaphore_signal(barrier, inc=1, device_id={axis: index}, device_id_type=MESH)

        when(valid, signal)
        total = total + (1 if valid is True else valid.astype(jnp.int32))
    pl.semaphore_wait(barrier, total)


def line_spots(me, grid):
    outer, inner = grid
    row, col = me // inner, me % inner
    spots = []
    if outer > 1:
        spots += [(row + 1 < outer, me + inner), (row > 0, me - inner)]
    if inner > 1:
        spots += [(col + 1 < inner, me + 1), (col > 0, me - 1)]
    return spots


def gather_kernel(axis, grid, pieces, count, *refs):
    ins, outs = refs[:count], refs[count : 2 * count]
    local_sem, send_sem, recv_sem = refs[2 * count :]
    outer, inner = grid
    me = lax.axis_index(axis)
    row, col = me // inner, me % inner
    locals_ = [pltpu.make_async_copy(ins[k], outs[k].at[me], local_sem.at[k]) for k in range(count)]
    for copy in locals_:
        copy.start()
    greet(axis, line_spots(me, grid))
    sends = []

    def copy_of(p, block, spot, target, own):
        k, start, rows, _ = pieces[p]
        here = outs[k].at[block, pl.ds(start, rows)]
        source = ins[k].at[pl.ds(start, rows)] if own else here
        return pltpu.make_async_remote_copy(
            src_ref=source,
            dst_ref=here,
            send_sem=send_sem.at[p, block, spot],
            recv_sem=recv_sem.at[p, block],
            device_id={axis: target},
            device_id_type=MESH,
        )

    def push(p, block, spot, target, valid, own=False):
        sends.append((p, block, spot, target, valid, own))
        when(valid, lambda: copy_of(p, block, spot, target, own).start())

    def land(p, block, valid):
        when(valid, lambda: copy_of(p, block, 0, me, False).wait_recv())

    events = []
    for p, (_, _, _, outer_first) in enumerate(pieces):
        if outer_first:
            first, second, pos1, pos2, step1, step2 = outer, inner, row, col, inner, 1
        else:
            first, second, pos1, pos2, step1, step2 = inner, outer, col, row, 1, inner
        spread = [(1, 0), (-1, 1)]

        def fits(pos, size, shift):
            return jnp.logical_and(pos + shift < size, pos + shift >= 0)

        def start_second(p, block, valid, own=False, pos2=pos2, second=second, step2=step2):
            if second > 1:
                for sign, spot in spread:
                    push(p, block, 2 + spot, me + sign * step2, both(valid, fits(pos2, second, sign)), own)

        def opening(p=p, pos1=pos1, first=first, step1=step1, start_second=start_second):
            if first > 1:
                for sign, spot in spread:
                    push(p, me, spot, me + sign * step1, fits(pos1, first, sign), True)
            start_second(p, me, True, True)

        events.append((0, p, opening))
        for s in range(1, first):
            for sign, spot in spread:

                def arrive(p=p, s=s, sign=sign, spot=spot, pos1=pos1, first=first, step1=step1, start_second=start_second):
                    block = me - sign * s * step1
                    valid = fits(pos1, first, -sign * s)
                    land(p, block, valid)
                    if s + 1 < first:
                        push(p, block, spot, me + sign * step1, both(valid, fits(pos1, first, sign)))
                    start_second(p, block, valid)

                events.append((s, p, arrive))
        for s in range(first):
            for sign1 in (1, -1) if s else (1,):
                for t in range(1, second):
                    for sign, spot in spread:

                        def relay(p=p, s=s, sign1=sign1, t=t, sign=sign, spot=spot, pos1=pos1, pos2=pos2, first=first, second=second, step1=step1, step2=step2):
                            block = me - sign1 * s * step1 - sign * t * step2
                            valid = fits(pos2, second, -sign * t)
                            if s:
                                valid = both(valid, fits(pos1, first, -sign1 * s))
                            land(p, block, valid)
                            if t + 1 < second:
                                push(p, block, 2 + spot, me + sign * step2, both(valid, fits(pos2, second, sign)))

                        events.append((s + t, p, relay))
    for _, _, event in sorted(events, key=lambda e: e[:2]):
        event()
    for p, block, spot, target, valid, own in sends:
        when(valid, lambda p=p, block=block, spot=spot, target=target, own=own: copy_of(p, block, spot, target, own).wait_send())
    for copy in locals_:
        copy.wait()


def gather(arrays, axis, size, grid, pieces, collective_id):
    count = len(arrays)
    return pl.pallas_call(
        functools.partial(gather_kernel, axis, grid, pieces, count),
        out_shape=[jax.ShapeDtypeStruct((size, *a.shape), a.dtype) for a in arrays],
        in_specs=[VMEM_SPEC] * count,
        out_specs=[VMEM_SPEC] * count,
        scratch_shapes=[
            pltpu.SemaphoreType.DMA((count,)),
            pltpu.SemaphoreType.DMA((len(pieces), size, 4)),
            pltpu.SemaphoreType.DMA((len(pieces), size)),
        ],
        compiler_params=pltpu.CompilerParams(
            collective_id=collective_id, has_side_effects=True, vmem_limit_bytes=60000000
        ),
    )(*arrays)


def scatter_kernel(axis, grid, orders, count, *refs):
    ins, outs = refs[:count], refs[count : 2 * count]
    rest = refs[2 * count :]
    stores, sems = rest[: 5 * count], rest[5 * count :]
    outer, inner = grid
    me = lax.axis_index(axis)
    row, col = me // inner, me % inner
    greet(axis, line_spots(me, grid))
    sends = []

    def line(k, phase, own, buffers, size, pos, step, sem_pair):
        send_sem, recv_sem = sem_pair

        def copy_of(way, dest, source):
            sign = 1 if way == 0 else -1
            return pltpu.make_async_remote_copy(
                src_ref=source,
                dst_ref=buffers[way].at[dest],
                send_sem=send_sem.at[way, dest],
                recv_sem=recv_sem.at[way, dest],
                device_id={axis: me + sign * step},
                device_id_type=MESH,
            )

        def round_(i):
            for way in (0, 1):
                dest = size - 1 - i if way == 0 else i
                valid = pos < dest if way == 0 else pos > dest
                edge = pos == 0 if way == 0 else pos == size - 1

                def from_edge(way=way, dest=dest):
                    copy_of(way, dest, own(dest)).start()

                def from_inside(way=way, dest=dest):
                    slot = buffers[way].at[dest]
                    copy_of(way, dest, slot).wait_recv()
                    slot[...] += own(dest)[...]
                    copy_of(way, dest, slot).start()

                when(both(valid, edge), from_edge)
                if size > 2:
                    when(both(valid, jnp.logical_not(edge)), from_inside)
                sends.append((valid, lambda way=way, dest=dest: copy_of(way, dest, buffers[way].at[dest]).wait_send()))

        def finish(total):
            total[...] = own(pos)[...]
            for way in (0, 1):

                def add(way=way):
                    slot = buffers[way].at[pos]
                    copy_of(way, pos, slot).wait_recv()
                    total[...] += slot[...]

                when(pos > 0 if way == 0 else pos < size - 1, add)

        return round_, finish

    jobs = []
    for k in range(count):
        up1, down1, middle, up2, down2 = stores[5 * k : 5 * k + 5]
        sem1, sem2 = sems[4 * k : 4 * k + 2], sems[4 * k + 2 : 4 * k + 4]
        ref = ins[k]
        if orders[k]:
            own1 = lambda d, ref=ref: ref.at[d]
            args1, args2 = (outer, row, inner), (inner, col, 1)
        else:
            own1 = lambda d, ref=ref: ref.at[:, d]
            args1, args2 = (inner, col, 1), (outer, row, inner)
        own2 = lambda d, middle=middle: middle.at[d]
        round1, finish1 = line(k, 0, own1, (up1, down1), *args1, sem1)
        round2, finish2 = line(k, 1, own2, (up2, down2), *args2, sem2)
        jobs.append((round1, finish1, round2, finish2, args1[0], args2[0], middle, outs[k]))
    span = max(j[4] for j in jobs) - 1 + max(j[5] for j in jobs)
    done = set()
    for tick in range(2 * (outer + inner)):
        for k, (round1, finish1, round2, finish2, size1, size2, middle, out) in enumerate(jobs):
            if tick < size1 - 1:
                round1(tick)
            elif tick == size1 - 1:
                finish1(middle)
                if size2 > 1:
                    round2(0)
            elif tick - size1 + 1 < size2 - 1:
                round2(tick - size1 + 1)
            elif k not in done:
                finish2(out)
                done.add(k)
    for valid, wait in sends:
        when(valid, wait)


def scatter(arrays, axis, grid, orders, collective_id):
    count = len(arrays)
    stores, sems = [], []
    for a, outer_first in zip(arrays, orders):
        outer, inner, rows, cols = a.shape
        first, second = (outer, inner) if outer_first else (inner, outer)
        stores += [pltpu.VMEM((first, second, rows, cols), a.dtype)] * 2
        stores += [pltpu.VMEM((second, rows, cols), a.dtype)] * 3
        sems += [pltpu.SemaphoreType.DMA((2, first))] * 2 + [pltpu.SemaphoreType.DMA((2, second))] * 2
    return pl.pallas_call(
        functools.partial(scatter_kernel, axis, grid, orders, count),
        out_shape=[jax.ShapeDtypeStruct(a.shape[2:], a.dtype) for a in arrays],
        in_specs=[VMEM_SPEC] * count,
        out_specs=[VMEM_SPEC] * count,
        scratch_shapes=stores + sems,
        compiler_params=pltpu.CompilerParams(
            collective_id=collective_id, has_side_effects=True, vmem_limit_bytes=60000000
        ),
    )(*arrays)


def total_kernel(sizes, x_ref, out_ref, near, far, mid, send_near, recv_near, send_far, recv_far):
    barrier = pltpu.get_barrier_semaphore()
    places = [("tp", sizes[1]), ("fs", sizes[0])]
    for axis, size in places:
        me = lax.axis_index(axis)
        for j in range(1, size):
            pl.semaphore_signal(barrier, inc=1, device_id={axis: (me + j) % size}, device_id_type=MESH)
    pl.semaphore_wait(barrier, sizes[0] + sizes[1] - 2)
    source = x_ref
    for (axis, size), held, send, recv, target in (
        (places[0], near, send_near, recv_near, mid),
        (places[1], far, send_far, recv_far, out_ref),
    ):
        me = lax.axis_index(axis)

        def copy_of(j, sign):
            return pltpu.make_async_remote_copy(
                src_ref=source,
                dst_ref=held.at[j],
                send_sem=send.at[j],
                recv_sem=recv.at[j],
                device_id={axis: (me + j) % size},
                device_id_type=MESH,
            )

        copies = [copy_of(j, 1) for j in range(1, size)]
        for copy in copies:
            copy.start()
        total = source[...]
        for j, copy in enumerate(copies, 1):
            copy.wait_recv()
            total = total + held[j]
        target[...] = total
        for copy in copies:
            copy.wait_send()
        source = mid


def total_over(x, sizes, collective_id):
    fs, tp = sizes
    return pl.pallas_call(
        functools.partial(total_kernel, sizes),
        out_shape=jax.ShapeDtypeStruct(x.shape, x.dtype),
        in_specs=[VMEM_SPEC],
        out_specs=VMEM_SPEC,
        scratch_shapes=[
            pltpu.VMEM((tp, *x.shape), x.dtype),
            pltpu.VMEM((fs, *x.shape), x.dtype),
            pltpu.VMEM(x.shape, x.dtype),
            pltpu.SemaphoreType.DMA((tp,)),
            pltpu.SemaphoreType.DMA((tp,)),
            pltpu.SemaphoreType.DMA((fs,)),
            pltpu.SemaphoreType.DMA((fs,)),
        ],
        compiler_params=pltpu.CompilerParams(collective_id=collective_id, has_side_effects=True),
    )(x)


def exact_dot(a, b):
    return jnp.dot(
        a.astype(jnp.float32), b.astype(jnp.float32), precision=lax.Precision.HIGHEST, preferred_element_type=jnp.float32
    )


def moments(first, second, proj):
    moment = BETA_ONE * first + (1.0 - BETA_ONE) * proj
    second_new = BETA_TWO * second + (1.0 - BETA_TWO) * proj * proj
    return moment, second_new, moment / jnp.sqrt(second_new)


def whole_rows(block):
    return (0, block.shape[0])


def on_device(
    fs, tp, h_saved, y_saved, d_gate, d_out, p_gate, p_out, w_gate, w_out, m_gate, m_out, v_gate, v_out
):
    fs_grid, tp_grid = grid_of(fs), (tp // CORES, CORES)
    rank = p_gate.shape[1]
    share = rank // tp
    mine = lax.axis_index("tp") * share
    slices = [lax.dynamic_slice_in_dim(p.T, mine, share, axis=0) for p in (p_gate, p_out)]
    wide = gather(slices, "fs", fs, fs_grid, ((0, 0, share, True), (1, 0, share, False)), 1)
    reduced = [
        lax.dot_general(
            jnp.transpose(g, (1, 0, 2)).reshape(share, -1),
            saved,
            (((1,), (1,)), ((), ())),
            preferred_element_type=jnp.float32,
        )
        for g, saved in zip(wide, (h_saved, y_saved))
    ]
    reduced = gather(reduced, "tp", tp, tp_grid, ((0, 0, share, True), (1, 0, share, True)), 2)
    parts = [
        exact_dot(r.reshape(rank, -1), d).reshape(*fs_grid, rank // fs, -1)
        for r, d in zip(reduced, (d_gate, d_out))
    ]
    proj_gate, proj_out = scatter(parts, "fs", fs_grid, (True, False), 3)
    moment_gate, second_gate, normed_gate = moments(m_gate, v_gate, proj_gate)
    moment_out, second_out, normed_out = moments(m_out, v_out, proj_out)
    rows = rank // fs
    whole = gather([normed_gate, normed_out], "fs", fs, fs_grid, ((0, 0, rows, False), (1, 0, rows, True)), 4)
    update_gate = exact_dot(p_gate, whole[0].reshape(rank, -1))
    update_out = exact_dot(p_out, whole[1].reshape(rank, -1))
    squares = jnp.concatenate(
        [jnp.full((8, 128), jnp.sum(u * u), jnp.float32) for u in (update_gate, update_out)], axis=0
    )
    squares = total_over(squares, (fs, tp), 5)
    step_gate = update_gate * lax.rsqrt(squares[0, 0] / (update_gate.size * fs * tp) + EPSILON)
    step_out = update_out * lax.rsqrt(squares[8, 0] / (update_out.size * fs * tp) + EPSILON)
    local_gate = (w_gate - LEARN_RATE * step_gate).astype(jnp.bfloat16)
    local_out = (w_out - LEARN_RATE * step_out).astype(jnp.bfloat16)
    half_gate, half_out = local_gate.shape[0] // 2, local_out.shape[0] // 2
    copies = gather(
        [local_gate, local_out],
        "fs",
        fs,
        fs_grid,
        ((0, 0, half_gate, False), (0, half_gate, half_gate, True), (1, 0, half_out, True), (1, half_out, half_out, True)),
        6,
    )
    copy_gate = copies[0].reshape(-1, local_gate.shape[1])
    copy_out = copies[1].reshape(-1, local_out.shape[1])
    return (step_gate, step_out, moment_gate, moment_out, second_gate, second_out, copy_gate, copy_out)


def solution(mesh):
    both_axes, rows = P("fs", "tp"), P("fs", None)
    fs, tp = mesh.shape["fs"], mesh.shape["tp"]
    return jax.shard_map(
        functools.partial(on_device, fs, tp),
        mesh=mesh,
        in_specs=(rows, rows, both_axes, both_axes, rows, rows) + (both_axes,) * 6,
        out_specs=(both_axes,) * 6 + (P(None, "tp"),) * 2,
        check_vma=False,
    )
```

time: 488 us -> 242 us (0.50)
  waiting for transfers between devices: 355 us -> 0 us
  Pallas kernels: 0 us -> 197 us
  blocking collectives: 70.4 us -> 0 us
  between operations: 15.6 us -> 2.22 us
    all_gather x5 -> x0, waiting for transfers between devices: 230 us -> none  [the longest x2 90.3 us: projected_partial(): lax.all_gather(factor, 'fs', axis=0, tiled=True)]
    pallas_call x0 -> x6, Pallas kernels: none -> 197 us  [the longest x4 148 us: gather(): pl.pallas_call(functools.partial(gather_kernel, axis, grid, pieces, count...]
    reduce_scatter x2 -> x0, waiting for transfers between devices: 123 us -> none  [the longest x1 62.3 us: on_device(): lax.psum_scatter(part_gate, 'fs', scatter_dimension=0, tiled=True)]
    psum x1 -> x0, blocking collectives: 38.7 us -> none  [on_device(): lax.psum((jnp.sum(update_gate * update_gate), jnp.sum(update_out * update...]
    all_gather x1 -> x0, blocking collectives: 31.7 us -> none  [on_device(): lax.all_gather(normed_gate, 'fs', axis=0, tiled=True)]
    unnamed x18 -> x30, local copies, waits for them, and re-layouts: 21.8 us -> 8.16 us
  transfers between devices with their start and end apart: 7 -> 0, of which waited for: 7 -> 0; matrix products, arithmetic and copies ran while one was open for 7% -> 0% of each run, Pallas kernels for 0% -> 0%
where the time goes in v1:
time: 242 us; the launch traced here: 241 us
  Pallas kernels  197 us (81%)
  local copies, waits for them, and re-layouts  17.3 us (7%)
  matrix products  16.7 us (7%)
  other arithmetic  7.58 us (3%)
    pallas_call x4, Pallas kernels, gather(): pl.pallas_call(functools.partial(gather_kernel, axis, grid, pieces, count...  148 us
    pallas_call x1, Pallas kernels, scatter(): pl.pallas_call(functools.partial(scatter_kernel, axis, grid, orders, coun...  39.5 us
    dot_general x4, matrix products, exact_dot(): jnp.dot(a.astype(jnp.float32), b.astype(jnp.float32), precision=lax.Preci...  10.9 us
    pallas_call x1, Pallas kernels, total_over(): pl.pallas_call(functools.partial(total_kernel, sizes), out_shape=jax.Shap...  10 us
    unnamed x30, local copies, waits for them, and re-layouts  8.16 us
    dot_general x2, matrix products, on_device(): lax.dot_general(jnp.transpose(g, (1, 0, 2)).reshape(share, -1), saved, ((...  5.79 us

profile of v1, /device:TPU:0, one launch (start us, length us, event | category | flops | bytes accessed | tf_op | source)
XLA Modules:
  0.0 241.0 jit_solution(17269445865829520723)
XLA Ops:
  0.6 0.0 copy-start
  0.7 1.1 constant_dynamic-slice_fusion
  1.7 0.7 copy.33
  2.4 1.0 constant_dynamic-slice_fusion.1
  3.5 0.7 copy.32
  4.2 20.4 %shard_map.179 = (bf16[8,64,512]{2,1,0:T(8,128)(2,1)}, bf16[8,64,256]{2,1,0:T(8,128)(2,1)}) custom-call(bf16[64,512]{1,0:T(8,128)(2,1)} %bitcast.51, bf16[64,256]{1,0:T(8,128)(2,1)} %bitcast.53), custom_call_target="tpu_custom_call" | custom-call | tf_op jit(solution)/shard_map/pallas_call | solution.py:155
  24.6 0.0 copy-start.8
  24.6 1.1 copy.34
  25.8 0.0 copy-start.6
  25.8 0.0 copy-start.3
  25.8 4.4 %fusion.9.refs_0_ = f32[64,512]{1,0:T(8,128)} fusion(bf16[64,4096]{1,0:T(8,128)(2,1)S(1)} %bitcast.44, bf16[512,4096]{1,0:T(8,128)(2,1)} %param.12), kind=kOutput, calls=%fused_computation.21 | convolution fusion | flops 268435456 | bytes 4849664 | tf_op jit(solution)/shard_map/dot_general | solution.py:367
  30.2 0.0 copy-done.8
  30.2 0.0 copy-done
  30.2 0.0 copy-start.11
  30.2 0.0 copy-start.12
  30.2 1.4 fusion.10.refs_1_
  31.6 0.0 copy-start.9
  31.6 0.0 copy-start.10
  31.7 0.0 copy-start.7
  31.7 12.2 %shard_map.180 = (f32[4,64,512]{2,1,0:T(8,128)}, f32[4,64,512]{2,1,0:T(8,128)}) custom-call(f32[64,512]{1,0:T(8,128)} %fusion.9.refs_0_, f32[64,512]{1,0:T(8,128)} %fusion.10.refs_1_), custom_call_target="tpu_custom_call" | custom-call | tf_op jit(solution)/shard_map/pallas_call | solution.py:155
  43.8 0.0 copy-done.6
  43.8 2.4 %fusion.2.refs_0_ = f32[4,2,32,512]{3,2,1,0:T(8,128)} fusion(f32[4,2,32,512]{3,2,1,0:T(8,128)} %bitcast.48, bf16[512,512]{1,0:T(8,128)(2,1)S(1)} %copy-done.6), kind=kOutput, calls=%fused_computation.8 | convolution fusion | flops 805306368 | bytes 1572864 | tf_op jit(solution)/shard_map/dot_general | solution.py:342
  46.2 0.0 copy-done.3
  46.2 3.0 %fusion.refs_1_ = f32[4,2,32,1024]{3,2,1,0:T(8,128)} fusion(f32[4,2,32,512]{3,2,1,0:T(8,128)} %bitcast.45, bf16[512,1024]{1,0:T(8,128)(2,1)S(1)} %copy-done.3), kind=kOutput, calls=%fused_computation | convolution fusion | flops 1610612736 | bytes 2621440 | tf_op jit(solution)/shard_map/dot_general | solution.py:342
  49.3 0.0 copy-start.5
  49.3 39.5 %shard_map.181 = (f32[32,512]{1,0:T(8,128)}, f32[32,1024]{1,0:T(8,128)}) custom-call(f32[4,2,32,512]{3,2,1,0:T(8,128)} %fusion.2.refs_0_, f32[4,2,32,1024]{3,2,1,0:T(8,128)} %fusion.refs_1_), custom_call_target="tpu_custom_call" | custom-call | tf_op jit(solution)/shard_map/pallas_call | solution.py:271
  88.7 0.0 copy-done.11
  88.8 0.0 copy-done.12
  88.8 1.5 rsqrt_multiply_fusion.1
  90.3 0.0 copy-done.9
  90.3 0.0 copy-done.10
  90.3 1.7 rsqrt_multiply_fusion
  92.0 21.3 %shard_map.182 = (f32[8,32,512]{2,1,0:T(8,128)}, f32[8,32,1024]{2,1,0:T(8,128)}) custom-call(f32[32,512]{1,0:T(8,128)} %get-tuple-element.35.refs_0_, f32[32,1024]{1,0:T(8,128)} %get-tuple-element.32.refs_1_), custom_call_target="tpu_custom_call" | custom-call | tf_op jit(solution)/shard_map/pallas_call | solution.py:155
  113.2 0.0 copy-done.7
  113.3 2.8 %multiply_reduce_fusion = (f32[]{:T(128)}, f32[1024,256]{1,0:T(8,128)S(1)}) fusion(f32[256,1024]{1,0:T(8,128)} %bitcast.46, bf16[256,256]{1,0:T(8,128)(2,1)S(1)} %copy-done.7), kind=kOutput, calls=%fused_computation.6 | convolution fusion | flops 805830656 | bytes 2228228 | tf_op jit(solution)/shard_map/dot_general | solution.py:342
  116.1 1.3 copy.29
  117.4 0.0 copy-done.5
  117.4 2.6 %multiply_reduce_fusion.1 = (f32[]{:T(128)}, f32[512,512]{1,0:T(8,128)S(1)}) fusion(f32[256,512]{1,0:T(8,128)} %bitcast.50, bf16[512,256]{1,0:T(8,128)(2,1)S(1)} %copy-done.5), kind=kOutput, calls=%fused_computation.7 | convolution fusion | flops 805830656 | bytes 1835012 | tf_op jit(solution)/shard_map/dot_general | solution.py:342
  120.1 1.3 copy.28
  121.4 0.0 copy-start.2
  121.4 0.7 broadcast_in_dim.4
  122.1 0.7 concatenate.5
  122.8 0.7 concatenate.6.x_ref
  123.4 10.0 %shard_map.183 = f32[16,128]{1,0:T(8,128)} custom-call(f32[16,128]{1,0:T(8,128)} %concatenate.6.x_ref), custom_call_target="tpu_custom_call" | custom-call | tf_op jit(solution)/shard_map/pallas_call | solution.py:323
  133.5 0.0 copy-start.4
  133.5 1.3 fusion.8
  136.2 3.0 %subtract_convert_fusion = (bf16[256,1024]{1,0:T(8,128)(2,1)}, f32[256,1024]{1,0:T(8,128)}) fusion(f32[256,1024]{1,0:T(8,128)} %param.19, f32[1024,256]{0,1:T(8,128)} %copy.29, f32[]{:T(128)} %bitcast.14), kind=kLoop, calls=%fused_computation.2 | loop fusion | flops 1048576 | bytes 3670020 | tf_op jit(solution)/shard_map/convert_element_type | solution.py:394
  139.2 0.0 copy-done.2
  139.2 0.0 copy-done.4
  139.2 1.4 subtract_convert_fusion.1
  140.6 93.8 %shard_map.184 = (bf16[8,512,512]{2,1,0:T(8,128)(2,1)}, bf16[8,256,1024]{2,1,0:T(8,128)(2,1)}) custom-call(bf16[512,512]{1,0:T(8,128)(2,1)} %get-tuple-element.30.refs_0_, bf16[256,1024]{1,0:T(8,128)(2,1)} %get-tuple-element.28.refs_1_), custom_call_target="tpu_custom_call" | custom-call | tf_op jit(solution)/shard_map/pallas_call | solution.py:155
  234.4 0.0 copy-start.1
  234.4 4.6 %copy.38 = bf16[4096,512]{1,0:T(8,128)(2,1)} copy(bf16[4096,512]{1,0:T(8,128)(2,1)} %bitcast.43) | data formatting | bytes 8388608
  239.0 0.0 copy-done.1
  239.0 2.0 copy.39
  (1 shorter events, 0.0 us)
Async XLA Ops:
  0.6 29.6 %copy-start = (bf16[512,2048]{1,0:T(8,128)(2,1)S(1)}, bf16[512,2048]{1,0:T(8,128)(2,1)}, u32[]{:S(2)}) copy-start(bf16[512,2048]{1,0:T(8,128)(2,1)} %param.13) | copy-start | bytes 6291460
  24.6 5.5 %copy-start.8 = (bf16[8,64,256]{2,1,0:T(8,128)(2,1)S(1)}, bf16[8,64,256]{2,1,0:T(8,128)(2,1)}, u32[]{:S(2)}) copy-start(bf16[8,64,256]{2,1,0:T(8,128)(2,1)} %get-tuple-element.19) | copy-start | bytes 786436
  25.8 18.0 %copy-start.6 = (bf16[512,512]{1,0:T(8,128)(2,1)S(1)}, bf16[512,512]{1,0:T(8,128)(2,1)}, u32[]{:S(2)}) copy-start(bf16[512,512]{1,0:T(8,128)(2,1)} %param.14) | copy-start | bytes 1572868
  25.8 20.5 %copy-start.3 = (bf16[512,1024]{1,0:T(8,128)(2,1)S(1)}, bf16[512,1024]{1,0:T(8,128)(2,1)}, u32[]{:S(2)}) copy-start(bf16[512,1024]{1,0:T(8,128)(2,1)} %param.15) | copy-start | bytes 3145732
  30.2 58.5 %copy-start.11 = (f32[32,512]{1,0:T(8,128)S(1)}, f32[32,512]{1,0:T(8,128)}, u32[]{:S(2)}) copy-start(f32[32,512]{1,0:T(8,128)} %param.22) | copy-start | bytes 196612
  30.2 58.5 %copy-start.12 = (f32[32,512]{1,0:T(8,128)S(1)}, f32[32,512]{1,0:T(8,128)}, u32[]{:S(2)}) copy-start(f32[32,512]{1,0:T(8,128)} %param.20) | copy-start | bytes 196612
  31.6 58.6 %copy-start.9 = (f32[32,1024]{1,0:T(8,128)S(1)}, f32[32,1024]{1,0:T(8,128)}, u32[]{:S(2)}) copy-start(f32[32,1024]{1,0:T(8,128)} %param.23) | copy-start | bytes 393220
  31.6 58.6 %copy-start.10 = (f32[32,1024]{1,0:T(8,128)S(1)}, f32[32,1024]{1,0:T(8,128)}, u32[]{:S(2)}) copy-start(f32[32,1024]{1,0:T(8,128)} %param.21) | copy-start | bytes 393220
  31.7 81.6 %copy-start.7 = (bf16[256,256]{1,0:T(8,128)(2,1)S(1)}, bf16[256,256]{1,0:T(8,128)(2,1)}, u32[]{:S(2)}) copy-start(bf16[256,256]{1,0:T(8,128)(2,1)} %param.17) | copy-start | bytes 393220
  49.3 68.1 %copy-start.5 = (bf16[512,256]{1,0:T(8,128)(2,1)S(1)}, bf16[512,256]{1,0:T(8,128)(2,1)}, u32[]{:S(2)}) copy-start(bf16[512,256]{1,0:T(8,128)(2,1)} %param.16) | copy-start | bytes 786436
  121.4 17.8 %copy-start.2 = (f32[512,512]{0,1:T(8,128)S(1)}, f32[512,512]{0,1:T(8,128)}, u32[]{:S(2)}) copy-start(f32[512,512]{0,1:T(8,128)} %copy.28) | copy-start | bytes 3145732
  133.5 5.7 %copy-start.4 = (f32[512,512]{1,0:T(8,128)S(1)}, f32[512,512]{1,0:T(8,128)}, u32[]{:S(2)}) copy-start(f32[512,512]{1,0:T(8,128)} %param.18) | copy-start | bytes 3145732
  234.4 4.6 %copy-start.1 = (bf16[8,256,1024]{2,1,0:T(8,128)(2,1)S(1)}, bf16[8,256,1024]{2,1,0:T(8,128)(2,1)}, u32[]{:S(2)}) copy-start(bf16[8,256,1024]{2,1,0:T(8,128)(2,1)} %get-tuple-element.27) | copy-start | bytes 12582916

commit v2 on v1

--- a/solution.py
+++ b/solution.py
@@ -63,19 +63,26 @@
 def gather_kernel(axis, grid, pieces, count, *refs):
     ins, outs = refs[:count], refs[count : 2 * count]
     local_sem, send_sem, recv_sem = refs[2 * count :]
-    outer, inner = grid
     me = lax.axis_index(axis)
-    row, col = me // inner, me % inner
     locals_ = [pltpu.make_async_copy(ins[k], outs[k].at[me], local_sem.at[k]) for k in range(count)]
     for copy in locals_:
         copy.start()
     greet(axis, line_spots(me, grid))
+    gather_rounds(axis, grid, pieces, ins, outs, send_sem, recv_sem)
+    for copy in locals_:
+        copy.wait()
+
+
+def gather_rounds(axis, grid, pieces, ins, outs, send_sem, recv_sem, beside=None):
+    outer, inner = grid
+    me = lax.axis_index(axis)
+    row, col = me // inner, me % inner
     sends = []
 
     def copy_of(p, block, spot, target, own):
         k, start, rows, _ = pieces[p]
         here = outs[k].at[block, pl.ds(start, rows)]
-        source = ins[k].at[pl.ds(start, rows)] if own else here
+        source = ins[k].at[pl.ds(start, rows)] if own and ins else here
         return pltpu.make_async_remote_copy(
             src_ref=source,
             dst_ref=here,
@@ -142,12 +149,12 @@
                                 push(p, block, 2 + spot, me + sign * step2, both(valid, fits(pos2, second, sign)))
 
                         events.append((s + t, p, relay))
+    if beside is not None:
+        events.append((0, len(pieces), beside))
     for _, _, event in sorted(events, key=lambda e: e[:2]):
         event()
     for p, block, spot, target, valid, own in sends:
         when(valid, lambda p=p, block=block, spot=spot, target=target, own=own: copy_of(p, block, spot, target, own).wait_send())
-    for copy in locals_:
-        copy.wait()
 
 
 def gather(arrays, axis, size, grid, pieces, collective_id):
@@ -168,10 +175,13 @@
     )(*arrays)
 
 
-def scatter_kernel(axis, grid, orders, count, *refs):
-    ins, outs = refs[:count], refs[count : 2 * count]
-    rest = refs[2 * count :]
-    stores, sems = rest[: 5 * count], rest[5 * count :]
+def scatter_kernel(axis, grid, parts, pieces, *refs):
+    ins, firsts, seconds = refs[:2], refs[2:4], refs[4:6]
+    moment_outs, second_outs, wholes = refs[6:8], refs[8:10], refs[10:12]
+    rest = refs[12:]
+    count = len(parts)
+    stores, sems = rest[: 6 * count], rest[6 * count : 10 * count]
+    send_all, recv_all = rest[10 * count :]
     outer, inner = grid
     me = lax.axis_index(axis)
     row, col = me // inner, me % inner
@@ -226,24 +236,31 @@
         return round_, finish
 
     jobs = []
-    for k in range(count):
-        up1, down1, middle, up2, down2 = stores[5 * k : 5 * k + 5]
+    for k, (which, start, width, outer_first) in enumerate(parts):
+        up1, down1, middle, up2, down2, proj = stores[6 * k : 6 * k + 6]
         sem1, sem2 = sems[4 * k : 4 * k + 2], sems[4 * k + 2 : 4 * k + 4]
-        ref = ins[k]
-        if orders[k]:
-            own1 = lambda d, ref=ref: ref.at[d]
+        ref, cols = ins[which], pl.ds(start, width)
+        if outer_first:
+            own1 = lambda d, ref=ref, cols=cols: ref.at[d, :, :, cols]
             args1, args2 = (outer, row, inner), (inner, col, 1)
         else:
-            own1 = lambda d, ref=ref: ref.at[:, d]
+            own1 = lambda d, ref=ref, cols=cols: ref.at[:, d, :, cols]
             args1, args2 = (inner, col, 1), (outer, row, inner)
         own2 = lambda d, middle=middle: middle.at[d]
         round1, finish1 = line(k, 0, own1, (up1, down1), *args1, sem1)
         round2, finish2 = line(k, 1, own2, (up2, down2), *args2, sem2)
-        jobs.append((round1, finish1, round2, finish2, args1[0], args2[0], middle, outs[k]))
-    span = max(j[4] for j in jobs) - 1 + max(j[5] for j in jobs)
+
+        def close(proj=proj, which=which, cols=cols, finish2=finish2):
+            finish2(proj)
+            moment, second, normed = moments(firsts[which][:, cols], seconds[which][:, cols], proj[...])
+            moment_outs[which][:, cols] = moment
+            second_outs[which][:, cols] = second
+            wholes[which][me, :, cols] = normed
+
+        jobs.append((round1, finish1, round2, close, args1[0], args2[0], middle))
     done = set()
     for tick in range(2 * (outer + inner)):
-        for k, (round1, finish1, round2, finish2, size1, size2, middle, out) in enumerate(jobs):
+        for k, (round1, finish1, round2, close, size1, size2, middle) in enumerate(jobs):
             if tick < size1 - 1:
                 round1(tick)
             elif tick == size1 - 1:
@@ -253,40 +270,58 @@
             elif tick - size1 + 1 < size2 - 1:
                 round2(tick - size1 + 1)
             elif k not in done:
-                finish2(out)
+                close()
                 done.add(k)
+    gather_rounds(axis, grid, pieces, None, wholes, send_all, recv_all)
     for valid, wait in sends:
         when(valid, wait)
 
 
-def scatter(arrays, axis, grid, orders, collective_id):
-    count = len(arrays)
+def scatter(arrays, firsts, seconds, axis, grid, parts, pieces, collective_id):
+    outer, inner = grid
+    size = outer * inner
     stores, sems = [], []
-    for a, outer_first in zip(arrays, orders):
-        outer, inner, rows, cols = a.shape
+    for which, _, width, outer_first in parts:
+        rows = arrays[which].shape[2]
         first, second = (outer, inner) if outer_first else (inner, outer)
-        stores += [pltpu.VMEM((first, second, rows, cols), a.dtype)] * 2
-        stores += [pltpu.VMEM((second, rows, cols), a.dtype)] * 3
+        stores += [pltpu.VMEM((first, second, rows, width), jnp.float32)] * 2
+        stores += [pltpu.VMEM((second, rows, width), jnp.float32)] * 3
+        stores += [pltpu.VMEM((rows, width), jnp.float32)]
         sems += [pltpu.SemaphoreType.DMA((2, first))] * 2 + [pltpu.SemaphoreType.DMA((2, second))] * 2
+    small = [jax.ShapeDtypeStruct(m.shape, m.dtype) for m in firsts]
+    wide = [jax.ShapeDtypeStruct((size, *m.shape), m.dtype) for m in firsts]
     return pl.pallas_call(
-        functools.partial(scatter_kernel, axis, grid, orders, count),
-        out_shape=[jax.ShapeDtypeStruct(a.shape[2:], a.dtype) for a in arrays],
-        in_specs=[VMEM_SPEC] * count,
-        out_specs=[VMEM_SPEC] * count,
-        scratch_shapes=stores + sems,
+        functools.partial(scatter_kernel, axis, grid, parts, pieces),
+        out_shape=small + small + wide,
+        in_specs=[VMEM_SPEC] * 6,
+        out_specs=[VMEM_SPEC] * 6,
+        scratch_shapes=stores
+        + sems
+        + [
+            pltpu.SemaphoreType.DMA((len(pieces), size, 4)),
+            pltpu.SemaphoreType.DMA((len(pieces), size)),
+        ],
         compiler_params=pltpu.CompilerParams(
             collective_id=collective_id, has_side_effects=True, vmem_limit_bytes=60000000
         ),
-    )(*arrays)
-
-
-def total_kernel(sizes, x_ref, out_ref, near, far, mid, send_near, recv_near, send_far, recv_far):
+    )(*arrays, *firsts, *seconds)
+
+
+def copies_kernel(sizes, grid, pieces, *refs):
+    updates, weights, steps, copies_ = refs[:2], refs[2:4], refs[4:6], refs[6:8]
+    x_ref, mid, out_ref, near, far = refs[8:13]
+    send_near, recv_near, send_far, recv_far, send_all, recv_all = refs[13:]
     barrier = pltpu.get_barrier_semaphore()
     places = [("tp", sizes[1]), ("fs", sizes[0])]
     for axis, size in places:
         me = lax.axis_index(axis)
         for j in range(1, size):
             pl.semaphore_signal(barrier, inc=1, device_id={axis: (me + j) % size}, device_id_type=MESH)
+    for k, update in enumerate(updates):
+        rows, cols = update.shape
+        value = update[...]
+        lanes = jnp.sum((value * value).reshape(rows // 8, 8, cols), axis=0)
+        x_ref[pl.ds(8 * k, 8), :] = sum(lanes[:, c : c + 128] for c in range(0, cols, 128))
     pl.semaphore_wait(barrier, sizes[0] + sizes[1] - 2)
     source = x_ref
     for (axis, size), held, send, recv, target in (
@@ -318,24 +353,49 @@
         source = mid
 
 
-def total_over(x, sizes, collective_id):
+    me = lax.axis_index("fs")
+    scales = []
+    for k, update in enumerate(updates):
+        total = jnp.sum(out_ref[pl.ds(8 * k, 8), :])
+        scales.append(lax.rsqrt(total / (update.shape[0] * update.shape[1] * sizes[0] * sizes[1]) + EPSILON))
+    for k, start, rows, _ in pieces:
+        held = pl.ds(start, rows)
+        step = updates[k][held, :] * scales[k]
+        copies_[k][me, held, :] = (weights[k][held, :] - LEARN_RATE * step).astype(jnp.bfloat16)
+
+    def write_steps():
+        for k, update in enumerate(updates):
+            steps[k][...] = update[...] * scales[k]
+
+    gather_rounds("fs", grid, pieces, None, copies_, send_all, recv_all, write_steps)
+
+
+def copies_of(updates, weights, sizes, grid, pieces, collective_id):
     fs, tp = sizes
+    tile = (16, 128)
     return pl.pallas_call(
-        functools.partial(total_kernel, sizes),
-        out_shape=jax.ShapeDtypeStruct(x.shape, x.dtype),
-        in_specs=[VMEM_SPEC],
-        out_specs=VMEM_SPEC,
+        functools.partial(copies_kernel, sizes, grid, pieces),
+        out_shape=[jax.ShapeDtypeStruct(u.shape, u.dtype) for u in updates]
+        + [jax.ShapeDtypeStruct((fs, *u.shape), jnp.bfloat16) for u in updates],
+        in_specs=[VMEM_SPEC] * 4,
+        out_specs=[VMEM_SPEC] * 4,
         scratch_shapes=[
-            pltpu.VMEM((tp, *x.shape), x.dtype),
-            pltpu.VMEM((fs, *x.shape), x.dtype),
-            pltpu.VMEM(x.shape, x.dtype),
+            pltpu.VMEM(tile, jnp.float32),
+            pltpu.VMEM(tile, jnp.float32),
+            pltpu.VMEM(tile, jnp.float32),
+            pltpu.VMEM((tp, *tile), jnp.float32),
+            pltpu.VMEM((fs, *tile), jnp.float32),
             pltpu.SemaphoreType.DMA((tp,)),
             pltpu.SemaphoreType.DMA((tp,)),
             pltpu.SemaphoreType.DMA((fs,)),
             pltpu.SemaphoreType.DMA((fs,)),
+            pltpu.SemaphoreType.DMA((len(pieces), fs, 4)),
+            pltpu.SemaphoreType.DMA((len(pieces), fs)),
         ],
-        compiler_params=pltpu.CompilerParams(collective_id=collective_id, has_side_effects=True),
-    )(x)
+        compiler_params=pltpu.CompilerParams(
+            collective_id=collective_id, has_side_effects=True, vmem_limit_bytes=60000000
+        ),
+    )(*updates, *weights)
 
 
 def exact_dot(a, b):
@@ -348,10 +408,6 @@
     moment = BETA_ONE * first + (1.0 - BETA_ONE) * proj
     second_new = BETA_TWO * second + (1.0 - BETA_TWO) * proj * proj
     return moment, second_new, moment / jnp.sqrt(second_new)
-
-
-def whole_rows(block):
-    return (0, block.shape[0])
 
 
 def on_device(
@@ -377,32 +433,39 @@
         exact_dot(r.reshape(rank, -1), d).reshape(*fs_grid, rank // fs, -1)
         for r, d in zip(reduced, (d_gate, d_out))
     ]
-    proj_gate, proj_out = scatter(parts, "fs", fs_grid, (True, False), 3)
-    moment_gate, second_gate, normed_gate = moments(m_gate, v_gate, proj_gate)
-    moment_out, second_out, normed_out = moments(m_out, v_out, proj_out)
     rows = rank // fs
-    whole = gather([normed_gate, normed_out], "fs", fs, fs_grid, ((0, 0, rows, False), (1, 0, rows, True)), 4)
-    update_gate = exact_dot(p_gate, whole[0].reshape(rank, -1))
-    update_out = exact_dot(p_out, whole[1].reshape(rank, -1))
-    squares = jnp.concatenate(
-        [jnp.full((8, 128), jnp.sum(u * u), jnp.float32) for u in (update_gate, update_out)], axis=0
+    wide_gate, wide_out = m_gate.shape[1], m_out.shape[1] // 2
+    moment_gate, moment_out, second_gate, second_out, whole_gate, whole_out = scatter(
+        parts,
+        (m_gate, m_out),
+        (v_gate, v_out),
+        "fs",
+        fs_grid,
+        ((0, 0, wide_gate, True), (1, 0, wide_out, False), (1, wide_out, wide_out, False)),
+        ((0, 0, rows, False), (1, 0, rows, True)),
+        3,
     )
-    squares = total_over(squares, (fs, tp), 5)
-    step_gate = update_gate * lax.rsqrt(squares[0, 0] / (update_gate.size * fs * tp) + EPSILON)
-    step_out = update_out * lax.rsqrt(squares[8, 0] / (update_out.size * fs * tp) + EPSILON)
-    local_gate = (w_gate - LEARN_RATE * step_gate).astype(jnp.bfloat16)
-    local_out = (w_out - LEARN_RATE * step_out).astype(jnp.bfloat16)
-    half_gate, half_out = local_gate.shape[0] // 2, local_out.shape[0] // 2
-    copies = gather(
-        [local_gate, local_out],
-        "fs",
-        fs,
+    updates = [
+        exact_dot(p, whole.reshape(rank, -1)) for p, whole in ((p_gate, whole_gate), (p_out, whole_out))
+    ]
+    half, quarter = w_gate.shape[0] // 2, w_out.shape[0] // 4
+    step_gate, step_out, copy_gate, copy_out = copies_of(
+        updates,
+        (w_gate, w_out),
+        (fs, tp),
         fs_grid,
-        ((0, 0, half_gate, False), (0, half_gate, half_gate, True), (1, 0, half_out, True), (1, half_out, half_out, True)),
-        6,
+        (
+            (1, 0, quarter, False),
+            (0, 0, half, True),
+            (0, half, half, True),
+            (1, quarter, quarter, True),
+            (1, 2 * quarter, quarter, True),
+            (1, 3 * quarter, quarter, True),
+        ),
+        5,
     )
-    copy_gate = copies[0].reshape(-1, local_gate.shape[1])
-    copy_out = copies[1].reshape(-1, local_out.shape[1])
+    copy_gate = copy_gate.reshape(-1, w_gate.shape[1])
+    copy_out = copy_out.reshape(-1, w_out.shape[1])
     return (step_gate, step_out, moment_gate, moment_out, second_gate, second_out, copy_gate, copy_out)
 
 

time: 242 us -> 231 us (0.955)
  other arithmetic: 7.58 us -> 0 us
    pallas_call x4 -> x2, Pallas kernels: 148 us -> 32.6 us  [gather(): pl.pallas_call(functools.partial(gather_kernel, axis, grid, pieces, count...]
    pallas_call x2, Pallas kernels: 49.5 us -> 163 us  [the longest x1 100 us: copies_of(): pl.pallas_call(functools.partial(copies_kernel, sizes, grid, pieces), out...]
    unnamed x30 -> x34, local copies, waits for them, and re-layouts: 8.16 us -> 14.5 us
    convert_element_type x2 -> x0, other arithmetic: 4.38 us -> none  [the longest x1 2.98 us: on_device(): local_out = (w_out - LEARN_RATE * step_out).astype(jnp.bfloat16)]
    div x2 -> x0, other arithmetic: 3.2 us -> none  [moments(): return (moment, second_new, moment / jnp.sqrt(second_new))]
    dot_general x2 -> x0, local copies, waits for them, and re-layouts: 2.61 us -> none  [exact_dot(): jnp.dot(a.astype(jnp.float32), b.astype(jnp.float32), precision=lax.Preci...]
where the time goes in v2:
time: 231 us
  Pallas kernels  195 us (84%)
  local copies, waits for them, and re-layouts  17.7 us (8%)
  matrix products  16.8 us (7%)
    pallas_call x1, Pallas kernels, copies_of(): pl.pallas_call(functools.partial(copies_kernel, sizes, grid, pieces), out...  100 us
    pallas_call x1, Pallas kernels, scatter(): pl.pallas_call(functools.partial(scatter_kernel, axis, grid, parts, piece...  62.4 us
    pallas_call x2, Pallas kernels, gather(): pl.pallas_call(functools.partial(gather_kernel, axis, grid, pieces, count...  32.6 us
    unnamed x34, local copies, waits for them, and re-layouts  14.5 us
    dot_general x4, matrix products, exact_dot(): jnp.dot(a.astype(jnp.float32), b.astype(jnp.float32), precision=lax.Preci...  11 us
    dot_general x2, matrix products, on_device(): lax.dot_general(jnp.transpose(g, (1, 0, 2)).reshape(share, -1), saved, ((...  5.79 us

profile of v2, /device:TPU:0, one launch (start us, length us, event | category | flops | bytes accessed | tf_op | source)
XLA Modules:
  0.0 230.6 jit_solution(18194892983256795669)
XLA Ops:
  0.6 0.0 copy-start
  0.7 1.1 constant_dynamic-slice_fusion
  1.7 0.7 copy.35
  2.4 1.0 constant_dynamic-slice_fusion.1
  3.5 0.7 copy.34
  4.2 20.5 %shard_map.179 = (bf16[8,64,512]{2,1,0:T(8,128)(2,1)}, bf16[8,64,256]{2,1,0:T(8,128)(2,1)}) custom-call(bf16[64,512]{1,0:T(8,128)(2,1)} %bitcast.47, bf16[64,256]{1,0:T(8,128)(2,1)} %bitcast.49), custom_call_target="tpu_custom_call" | custom-call | tf_op jit(solution)/shard_map/pallas_call | solution.py:162
  24.7 0.0 copy-start.7
  24.7 1.1 copy.36
  25.8 0.0 copy-start.5
  25.8 0.0 copy-start.3
  25.8 4.4 %fusion.4.refs_0_ = f32[64,512]{1,0:T(8,128)} fusion(bf16[64,4096]{1,0:T(8,128)(2,1)S(1)} %bitcast.40, bf16[512,4096]{1,0:T(8,128)(2,1)} %param.12), kind=kOutput, calls=%fused_computation.8 | convolution fusion | flops 268435456 | bytes 4849664 | tf_op jit(solution)/shard_map/dot_general | solution.py:423
  30.2 0.0 copy-done.7
  30.2 0.0 copy-done
  30.2 1.4 fusion.5.refs_1_
  31.6 0.0 copy-start.6
  31.6 12.1 %shard_map.180 = (f32[4,64,512]{2,1,0:T(8,128)}, f32[4,64,512]{2,1,0:T(8,128)}) custom-call(f32[64,512]{1,0:T(8,128)} %fusion.4.refs_0_, f32[64,512]{1,0:T(8,128)} %fusion.5.refs_1_), custom_call_target="tpu_custom_call" | custom-call | tf_op jit(solution)/shard_map/pallas_call | solution.py:162
  43.8 0.0 copy-done.5
  43.8 2.4 %fusion.2.refs_0_ = f32[4,2,32,512]{3,2,1,0:T(8,128)} fusion(f32[4,2,32,512]{3,2,1,0:T(8,128)} %bitcast.45, bf16[512,512]{1,0:T(8,128)(2,1)S(1)} %copy-done.5), kind=kOutput, calls=%fused_computation.4 | convolution fusion | flops 805306368 | bytes 1572864 | tf_op jit(solution)/shard_map/dot_general | solution.py:402
  46.2 0.0 copy-start.4
  46.2 0.0 copy-done.3
  46.2 3.1 %fusion.refs_1_ = f32[4,2,32,1024]{3,2,1,0:T(8,128)} fusion(f32[4,2,32,512]{3,2,1,0:T(8,128)} %bitcast.41, bf16[512,1024]{1,0:T(8,128)(2,1)S(1)} %copy-done.3), kind=kOutput, calls=%fused_computation.2 | convolution fusion | flops 1610612736 | bytes 2621440 | tf_op jit(solution)/shard_map/dot_general | solution.py:402
  49.3 62.4 %shard_map.181 = (f32[32,512]{1,0:T(8,128)}, f32[32,1024]{1,0:T(8,128)}, f32[32,512]{1,0:T(8,128)}, f32[32,1024]{1,0:T(8,128)}, f32[8,32,512]{2,1,0:T(8,128)}, /*index=5*/f32[8,32,1024]{2,1,0:T(8,128)}) custom-call(f32[4,2,32,512]{3,2,1,0:T(8,128)} %fusion.2.refs_0_, f32[4,2,32,1024]{3,2,1,0:T(8,128)} %fusion.refs_1_, f32[32,512]{1,0:T(8,128)} %refs_2_.2, ...), custom_call_target="tpu_custom_call" | custom-call | tf_op jit(solution)/shard_map/pallas_call | solution.py:293
  111.7 0.0 copy-done.6
  111.7 2.9 %convolution_bitcast_fusion.refs_1_ = f32[256,1024]{1,0:T(8,128)} fusion(f32[256,1024]{1,0:T(8,128)} %bitcast.43, bf16[256,256]{1,0:T(8,128)(2,1)S(1)} %copy-done.6), kind=kOutput, calls=%fused_computation | convolution fusion | flops 805306368 | bytes 2228224 | tf_op jit(solution)/shard_map/dot_general | solution.py:402
  114.5 0.0 copy-done.4
  114.6 2.6 %convolution_bitcast_fusion.1.refs_0_ = f32[512,512]{1,0:T(8,128)} fusion(f32[256,512]{1,0:T(8,128)} %bitcast.44, bf16[512,256]{1,0:T(8,128)(2,1)S(1)} %copy-done.4), kind=kOutput, calls=%fused_computation.1 | convolution fusion | flops 805306368 | bytes 1835008 | tf_op jit(solution)/shard_map/dot_general | solution.py:402
  117.2 0.0 copy-start.11
  117.2 0.0 copy-start.9
  117.2 0.0 copy-start.10
  117.2 0.0 copy-start.8
  117.2 100.3 %shard_map.182 = (f32[512,512]{1,0:T(8,128)}, f32[256,1024]{1,0:T(8,128)}, bf16[8,512,512]{2,1,0:T(8,128)(2,1)}, bf16[8,256,1024]{2,1,0:T(8,128)(2,1)}) custom-call(f32[512,512]{1,0:T(8,128)} %convolution_bitcast_fusion.1.refs_0_, f32[256,1024]{1,0:T(8,128)} %convolution_bitcast_fusion.refs_1_, f32[512,512]{1,0:T(8,128)} %refs_2_.3, f32[256,1024]{1,0:T(8,128)} %refs_3_.3), custom_call_target="tpu_custom_call" | custom-call | tf_op jit(solution)/shard_map/pallas_call | solution.py:376
  217.6 0.0 copy-start.2
  217.6 2.4 %copy.46 = f32[512,512]{1,0:T(8,128)} copy(f32[512,512]{1,0:T(8,128)} %get-tuple-element.44) | data formatting | bytes 2097152
  220.0 2.3 copy.47
  222.3 0.0 copy-done.11
  222.3 0.6 copy.48
  222.9 0.0 copy-done.9
  222.9 0.7 copy.49
  223.6 0.0 copy-done.10
  223.6 0.6 copy.50
  224.2 0.0 copy-done.8
  224.2 0.7 copy.51
  224.9 0.0 copy-done.2
  224.9 0.0 copy-start.1
  224.9 2.1 copy.52
  227.0 1.6 copy-done.1
  228.6 2.0 copy.53
  (1 shorter events, 0.0 us)
Async XLA Ops:
  0.6 29.6 %copy-start = (bf16[512,2048]{1,0:T(8,128)(2,1)S(1)}, bf16[512,2048]{1,0:T(8,128)(2,1)}, u32[]{:S(2)}) copy-start(bf16[512,2048]{1,0:T(8,128)(2,1)} %param.13) | copy-start | bytes 6291460
  24.7 5.5 %copy-start.7 = (bf16[8,64,256]{2,1,0:T(8,128)(2,1)S(1)}, bf16[8,64,256]{2,1,0:T(8,128)(2,1)}, u32[]{:S(2)}) copy-start(bf16[8,64,256]{2,1,0:T(8,128)(2,1)} %get-tuple-element.23) | copy-start | bytes 786436
  25.8 18.0 %copy-start.5 = (bf16[512,512]{1,0:T(8,128)(2,1)S(1)}, bf16[512,512]{1,0:T(8,128)(2,1)}, u32[]{:S(2)}) copy-start(bf16[512,512]{1,0:T(8,128)(2,1)} %param.14) | copy-start | bytes 1572868
  25.8 20.4 %copy-start.3 = (bf16[512,1024]{1,0:T(8,128)(2,1)S(1)}, bf16[512,1024]{1,0:T(8,128)(2,1)}, u32[]{:S(2)}) copy-start(bf16[512,1024]{1,0:T(8,128)(2,1)} %param.15) | copy-start | bytes 3145732
  31.6 80.0 %copy-start.6 = (bf16[256,256]{1,0:T(8,128)(2,1)S(1)}, bf16[256,256]{1,0:T(8,128)(2,1)}, u32[]{:S(2)}) copy-start(bf16[256,256]{1,0:T(8,128)(2,1)} %param.17) | copy-start | bytes 393220
  46.2 68.3 %copy-start.4 = (bf16[512,256]{1,0:T(8,128)(2,1)S(1)}, bf16[512,256]{1,0:T(8,128)(2,1)}, u32[]{:S(2)}) copy-start(bf16[512,256]{1,0:T(8,128)(2,1)} %param.16) | copy-start | bytes 786436
  117.2 105.1 %copy-start.11 = (f32[32,512]{1,0:T(8,128)S(1)}, f32[32,512]{1,0:T(8,128)}, u32[]{:S(2)}) copy-start(f32[32,512]{1,0:T(8,128)} %get-tuple-element.46) | copy-start | bytes 196612
  117.2 105.7 %copy-start.9 = (f32[32,1024]{1,0:T(8,128)S(1)}, f32[32,1024]{1,0:T(8,128)}, u32[]{:S(2)}) copy-start(f32[32,1024]{1,0:T(8,128)} %get-tuple-element.47) | copy-start | bytes 393220
  117.2 106.4 %copy-start.10 = (f32[32,512]{1,0:T(8,128)S(1)}, f32[32,512]{1,0:T(8,128)}, u32[]{:S(2)}) copy-start(f32[32,512]{1,0:T(8,128)} %get-tuple-element.48) | copy-start | bytes 196612
  117.2 107.0 %copy-start.8 = (f32[32,1024]{1,0:T(8,128)S(1)}, f32[32,1024]{1,0:T(8,128)}, u32[]{:S(2)}) copy-start(f32[32,1024]{1,0:T(8,128)} %get-tuple-element.49) | copy-start | bytes 393220
  217.6 7.3 %copy-start.2 = (bf16[8,512,512]{2,1,0:T(8,128)(2,1)S(1)}, bf16[8,512,512]{2,1,0:T(8,128)(2,1)}, u32[]{:S(2)}) copy-start(bf16[8,512,512]{2,1,0:T(8,128)(2,1)} %get-tuple-element.34) | copy-start | bytes 12582916
  224.9 3.7 %copy-start.1 = (bf16[8,256,1024]{2,1,0:T(8,128)(2,1)S(1)}, bf16[8,256,1024]{2,1,0:T(8,128)(2,1)}, u32[]{:S(2)}) copy-start(bf16[8,256,1024]{2,1,0:T(8,128)(2,1)} %get-tuple-element.35) | copy-start | bytes 12582916
